TPU v7x, 32 devices: a whole 2x2x4 slice. The times are simulated.
32 devices in a mesh: grp: 2 (over y), ep: 8 (over z, x), tp: 2 (over core).
Axes of the slice: x: 2, y: 2, z: 4, core: 2. Of those that a mesh axis runs over, the one named last changes fastest.
Arguments:
- tokens: bfloat16 [512, 1024], P(('grp', 'ep', 'tp')), parts along dimension 0, may hold values from -1.75 to 1.75
- latent_cache: bfloat16 [512, 1024, 256], P(('grp', 'ep', 'tp')), parts along dimension 0, may hold values from -6 to 6
- rope_cache: bfloat16 [512, 1024, 32], P(('grp', 'ep', 'tp')), parts along dimension 0, may hold values from -1200 to 1200
- lengths: int32 [512], P(('grp', 'ep', 'tp')), parts along dimension 0, may hold values from 128 to 1024
- expert_ids: int32 [512, 4], P(('grp', 'ep', 'tp')), parts along dimension 0, may hold values from 0 to 15, all different within a row; in each aligned block of 16 rows (0 to 15, 16 to 31, ...) at most 4 rows name the same one
- route_weights: float32 [512, 4], P(('grp', 'ep', 'tp')), parts along dimension 0, may hold values from 0.1 to 1
- g_attn: float32 [1024], replicated, may hold values from 0.1 to 1.9
- w_query_down: bfloat16 [1024, 256], replicated, may hold values from -0.1875 to 0.1875
- g_query: float32 [256], replicated, may hold values from 0.1 to 1.9
- w_latent_down: bfloat16 [1024, 256], replicated, may hold values from -0.1875 to 0.1875
- g_latent: float32 [256], replicated, may hold values from 0.1 to 1.9
- w_rope_key: bfloat16 [1024, 32], replicated, may hold values from -0.1875 to 0.1875
- w_query: bfloat16 [256, 1024], replicated, may hold values from -0.375 to 0.375
- w_query_rope: bfloat16 [256, 512], replicated, may hold values from -0.375 to 0.375
- w_key_up: bfloat16 [256, 1024], replicated, may hold values from -0.875 to 0.875
- w_value_up: bfloat16 [256, 1024], replicated, may hold values from -0.375 to 0.375
- w_out: bfloat16 [1024, 1024], replicated, may hold values from -0.1875 to 0.1875
- g_ffn: float32 [1024], replicated, may hold values from 0.1 to 1.9
- w_expert_gate: bfloat16 [16, 1024, 256], P('ep', None, 'tp'), may hold values from -0.1875 to 0.1875
- w_expert_up: bfloat16 [16, 1024, 256], P('ep', None, 'tp'), may hold values from -0.1875 to 0.1875
- w_expert_down: bfloat16 [16, 256, 1024], P('ep', 'tp'), may hold values from -0.375 to 0.375
- w_shared_gate: bfloat16 [1024, 256], replicated, may hold values from -0.1875 to 0.1875
- w_shared_up: bfloat16 [1024, 256], replicated, may hold values from -0.1875 to 0.1875
- w_shared_down: bfloat16 [256, 1024], replicated, may hold values from -0.375 to 0.375
Outputs:
- mixed_out: bfloat16 [512, 1024], P(('grp', 'ep', 'tp')), parts along dimension 0
- new_entry: bfloat16 [512, 288], P(('grp', 'ep', 'tp')), parts along dimension 0
There are 2 independent parts, one for each index of `grp`. A program takes and returns all parts, laid end to end along the dimension named above; an argument that names none is the same for every part. Nothing has to cross between parts.
Inputs may be any that keep to these rules, and one draw needn't show every extreme that they name: `expert_ids`: each row names 4 different experts. In the aligned blocks of rows that one device holds (one block for each device of ep and tp together), no expert is named by more than 4 rows, a bound that some block reaches.
All inputs are finite; a program needn't handle non-finite values.
Results may differ from a plain program's by a relative error of at most 0.03.
Values may be sent and summed in bfloat16 or wider, within the bound.
A program may use at most 64 MiB of HBM per device.

v0:
```python
import functools

import jax
import jax.numpy as jnp
from jax import lax
from jax.experimental import pallas as pl
from jax.experimental.pallas import tpu as pltpu
from jax.sharding import PartitionSpec as P

HEADS = 16
NOPE = 64
ROPE = 32
VDIM = 64
CAP = 4
GROUP = 8

norm_eps = 1e-06
masked_score = -1e30
F32 = jnp.float32
BF16 = jnp.bfloat16
MESH = pl.DeviceIdType.MESH


def nn(a, b):
    return jnp.dot(a, b, preferred_element_type=F32)


def nt(a, b):
    return lax.dot_general(a, b, (((1,), (1,)), ((), ())), preferred_element_type=F32)


def iota(shape, axis):
    return lax.broadcasted_iota(jnp.int32, shape, axis)


def rms(values, gain):
    mean_square = jnp.mean(values * values, axis=-1, keepdims=True)
    return values * lax.rsqrt(mean_square + norm_eps) * gain


def silu(v):
    return v / (1.0 + jnp.exp(-v))


def onehot(cond):
    return jnp.where(cond, 1.0, 0.0).astype(BF16)


def step_kernel(ep_size, tp_size, names, lens, *refs):
    count = len(names)
    hbm = dict(zip(names, refs[:count]))
    out_ref, entry_ref = refs[count : count + 2]
    refs = refs[count + 2 :]
    vmem = dict(zip(names, refs[:count]))
    (
        ql_ref,
        qr_ref,
        mix_ref,
        spread_ref,
        weight_ref,
        outbox,
        inbox,
        ret_out,
        ret_in,
        in_sem,
        cache_sem,
        rope_sem,
        swap_send,
        swap_recv,
        out_send,
        out_recv,
        back_send,
        back_recv,
        own_sem,
    ) = refs[count:]
    rows, width = hbm["tokens"].shape
    length = hbm["latent_cache"].shape[1]
    own_experts = vmem["w_expert_gate"].shape[1]
    devices = ep_size * tp_size
    block = own_experts * CAP
    slots = devices * block
    ep = lax.axis_index("ep")
    tp = lax.axis_index("tp")
    me = ep * tp_size + tp

    def ident(d):
        return {"ep": d // tp_size, "tp": d % tp_size}

    barrier = pltpu.get_barrier_semaphore()

    @pl.loop(1, devices)
    def _(i):
        pl.semaphore_signal(
            barrier, inc=1, device_id=ident(lax.rem(me + i, devices)), device_id_type=MESH
        )

    expert_names = ("w_expert_gate", "w_expert_up", "w_expert_down")

    def load(name):
        i = names.index(name)
        if name in expert_names:
            src = hbm[name].at[pl.ds(tp * own_experts, own_experts)]
            return pltpu.make_async_copy(src, vmem[name].at[tp], in_sem.at[i])
        return pltpu.make_async_copy(hbm[name], vmem[name], in_sem.at[i])

    def cache_copies(g):
        part = pl.ds(g * GROUP, GROUP)
        return (
            pltpu.make_async_copy(
                hbm["latent_cache"].at[part], vmem["latent_cache"].at[part], cache_sem.at[g]
            ),
            pltpu.make_async_copy(
                hbm["rope_cache"].at[part], vmem["rope_cache"].at[part], rope_sem.at[g]
            ),
        )

    groups = rows // GROUP
    early = (
        "expert_ids", "route_weights", "tokens", "g_attn", "g_query", "g_latent", "g_ffn",
        "w_query_down", "w_latent_down", "w_rope_key", "w_query", "w_query_rope", "w_key_up",
    )
    late = (
        "w_value_up", "w_out", "w_shared_gate", "w_shared_up", "w_shared_down",
    ) + expert_names
    for name in early:
        load(name).start()

    @pl.loop(0, groups)
    def _(g):
        for copy in cache_copies(g):
            copy.start()

    for name in late:
        load(name).start()

    def ready(name):
        load(name).wait()
        return vmem[name]

    ids = ready("expert_ids")[...]
    route = ready("route_weights")[...]
    slot = iota((slots, rows), 0)
    slot_expert = lax.shift_right_logical(slot, 2)
    named = jnp.zeros((slots, rows), F32)
    slot_weight = jnp.zeros((slots, rows), F32)
    for k in range(ids.shape[0]):
        hit = slot_expert == ids[k : k + 1, :]
        named = jnp.where(hit, 1.0, named)
        slot_weight = jnp.where(hit, route[k : k + 1, :], slot_weight)
    before = onehot(iota((rows, rows), 0) < iota((rows, rows), 1))
    rank = nn(named.astype(BF16), before)
    taken = jnp.logical_and(named > 0.5, rank == (slot & (CAP - 1)).astype(F32))
    spread_ref[...] = onehot(taken)
    slot_weight = jnp.where(taken, slot_weight, 0.0)
    high = slot_weight.astype(BF16)
    low = (slot_weight - high.astype(F32)).astype(BF16)
    eye = onehot(iota((rows, rows), 0) == iota((rows, rows), 1))
    weight_ref[0:rows, :] = nt(eye, high).astype(BF16)
    weight_ref[rows : 2 * rows, :] = nt(eye, low).astype(BF16)

    row_id = iota((rows, 128), 0)
    position = jnp.zeros((rows, 128), F32)
    for s in range(rows):
        position = jnp.where(row_id == s, lens[s].astype(F32), position)
    lane = iota((rows, 128), 1)
    half = ROPE // 2
    frequency = jnp.exp((lane & (half - 1)).astype(F32) * (-9.210340371976184 / half))
    angle = position * frequency
    cosine = jnp.cos(angle)
    sine = jnp.sin(angle)
    sine = jnp.where((lane & (ROPE - 1)) < half, -sine, sine)

    tokens = ready("tokens")[...].astype(F32)
    normed = rms(tokens, ready("g_attn")[...]).astype(BF16)
    gain_query = ready("g_query")[...]
    query_low = rms(nn(normed, ready("w_query_down")[...]), gain_query).astype(BF16)
    gain_latent = ready("g_latent")[...]
    latent_new = rms(nn(normed, ready("w_latent_down")[...]), gain_latent)
    key = nt(normed, ready("w_rope_key")[...])
    swapped = jnp.concatenate([key[:, half:], key[:, :half]], axis=1)
    key_new = key * cosine[:, :ROPE] + swapped * sine[:, :ROPE]
    kvl = latent_new.shape[1]
    entry_ref[:, 0:kvl] = latent_new.astype(BF16)
    entry_ref[:, kvl : kvl + ROPE] = key_new.astype(BF16)

    query = nn(query_low, ready("w_query")[...]).astype(BF16)
    turn = nn(query_low, ready("w_query_rope")[...])
    rope_width = turn.shape[1]
    rope_lane = iota((rows, rope_width), 1)
    swapped = jnp.where(
        (rope_lane & (ROPE - 1)) < half,
        pltpu.roll(turn, rope_width - half, 1),
        pltpu.roll(turn, half, 1),
    )
    tiles = rope_width // 128
    turned = (
        turn * jnp.concatenate([cosine] * tiles, axis=1)
        + swapped * jnp.concatenate([sine] * tiles, axis=1)
    ).astype(BF16)
    pairs = rows * HEADS
    repeat = onehot(lax.shift_right_logical(iota((pairs, rows), 0), 4) == iota((pairs, rows), 1))

    def head_mask(columns, shift):
        head = iota((pairs, columns), 0) & (HEADS - 1)
        return head == lax.shift_right_logical(iota((pairs, columns), 1), shift)

    nope_mask = head_mask(query.shape[1], 6)
    spread_query = jnp.where(nope_mask, nn(repeat, query), 0.0).astype(BF16)
    ql_ref[...] = nt(spread_query, ready("w_key_up")[...]).astype(BF16)
    spread_turn = jnp.where(head_mask(rope_width, 5), nn(repeat, turned), 0.0).astype(BF16)
    fold = onehot(
        (iota((rope_width, ROPE), 0) & (ROPE - 1)) == iota((rope_width, ROPE), 1)
    )
    qr_ref[...] = nn(spread_turn, fold).astype(BF16)

    swaps = []
    for p in range(1, tp_size):
        peer = lax.rem(tp + p, tp_size)
        for i, name in enumerate(expert_names):
            swaps.append(
                pltpu.make_async_remote_copy(
                    src_ref=hbm[name].at[pl.ds(peer * own_experts, own_experts)],
                    dst_ref=vmem[name].at[tp],
                    send_sem=swap_send.at[i, p],
                    recv_sem=swap_recv.at[i, p],
                    device_id={"tp": peer},
                    device_id_type=MESH,
                )
            )

    scale = (NOPE + ROPE) ** (-0.5)
    time_lane = iota((HEADS, length), 1)

    @pl.loop(0, groups)
    def _(g):
        for copy in cache_copies(g):
            copy.wait()
        parts = []
        scored = []
        for j in range(GROUP):
            s = g * GROUP + j
            part = pl.ds(pl.multiple_of(s * HEADS, HEADS), HEADS)
            parts.append((s, part))
            scores = nt(ql_ref[part, :], vmem["latent_cache"][s])
            scored.append(scores + nn(qr_ref[part, :], vmem["rope_cache"][s]))
        soft = []
        for (s, part), scores in zip(parts, scored):
            live = time_lane < lens[s]
            scores = jnp.where(live, scores * scale, masked_score)
            top = jnp.max(scores, axis=1, keepdims=True)
            weights = jnp.where(live, jnp.exp(scores - top), 0.0)
            soft.append((weights.astype(BF16), jnp.sum(weights, axis=1, keepdims=True)))
        for (s, part), (weights, total) in zip(parts, soft):
            mixed = nn(weights, vmem["latent_cache"][s])
            mix_ref[part, :] = (mixed / total).astype(BF16)

    pl.semaphore_wait(barrier, devices - 1)
    for copy in swaps:
        copy.start()

    heads_all = nn(mix_ref[...], ready("w_value_up")[...])
    heads_all = jnp.where(head_mask(heads_all.shape[1], 6), heads_all, 0.0).astype(BF16)
    gather = onehot(iota((rows, pairs), 0) == lax.shift_right_logical(iota((rows, pairs), 1), 4))
    value_heads = nn(gather, heads_all).astype(BF16)
    hidden = (tokens + nn(value_heads, ready("w_out")[...])).astype(BF16).astype(F32)
    normed_ffn = rms(hidden, ready("g_ffn")[...]).astype(BF16)

    box = nn(spread_ref[...], normed_ffn).astype(BF16)
    for d in range(devices):
        outbox[d] = box[d * block : (d + 1) * block, :]

    def own_copy(src, dst, i):
        return pltpu.make_async_copy(src.at[me], dst.at[me], own_sem.at[i])

    def post(src, dst, send, recv, d):
        return pltpu.make_async_remote_copy(
            src_ref=src.at[d],
            dst_ref=dst.at[me],
            send_sem=send.at[d],
            recv_sem=recv.at[me],
            device_id=ident(d),
            device_id_type=MESH,
        )

    def arrival(dst, send, recv, d):
        return pltpu.make_async_remote_copy(
            src_ref=dst.at[d],
            dst_ref=dst.at[d],
            send_sem=send.at[d],
            recv_sem=recv.at[d],
            device_id=ident(d),
            device_id_type=MESH,
        )

    def send_all(src, dst, send, recv, i):
        @pl.loop(1, devices)
        def _(step):
            post(src, dst, send, recv, lax.rem(me + step, devices)).start()

        own_copy(src, dst, i).start()

    def take_all(src, dst, send, recv, i):
        own_copy(src, dst, i).wait()

        @pl.loop(1, devices)
        def _(step):
            arrival(dst, send, recv, lax.rem(me + step, devices)).wait_recv()

    def drain(src, dst, send, recv):
        @pl.loop(1, devices)
        def _(step):
            post(src, dst, send, recv, lax.rem(me + step, devices)).wait_send()

    send_all(outbox, inbox, out_send, out_recv, 0)

    shared_gate = nn(normed_ffn, ready("w_shared_gate")[...])
    shared_up = nn(normed_ffn, ready("w_shared_up")[...])
    shared_hidden = (silu(shared_gate) * shared_up).astype(BF16)
    base = hidden + nn(shared_hidden, ready("w_shared_down")[...])
    for name in expert_names:
        load(name).wait()
    for copy in swaps:
        copy.wait()

    take_all(outbox, inbox, out_send, out_recv, 0)

    gates, ups, downs = (vmem[name] for name in expert_names)
    for e in range(own_experts):
        x = jnp.concatenate(
            [inbox[d, e * CAP : (e + 1) * CAP, :] for d in range(devices)], axis=0
        )
        total = jnp.zeros((devices * CAP, width), F32)
        for t in range(tp_size):
            unit = (silu(nn(x, gates[t, e])) * nn(x, ups[t, e])).astype(BF16)
            total = total + nn(unit, downs[t, e]).astype(BF16).astype(F32)
        total = total.astype(BF16)
        for d in range(devices):
            ret_out[d, e * CAP : (e + 1) * CAP, :] = total[d * CAP : (d + 1) * CAP, :]
    send_all(ret_out, ret_in, back_send, back_recv, 1)
    drain(outbox, inbox, out_send, out_recv)
    take_all(ret_out, ret_in, back_send, back_recv, 1)
    returned = jnp.concatenate([ret_in[d] for d in range(devices)], axis=0)
    both = nn(weight_ref[...], returned)
    out_ref[...] = (base + both[0:rows, :] + both[rows : 2 * rows, :]).astype(BF16)
    drain(ret_out, ret_in, back_send, back_recv)


NAMES = (
    "tokens", "latent_cache", "rope_cache", "expert_ids", "route_weights", "g_attn",
    "w_query_down", "g_query", "w_latent_down", "g_latent", "w_rope_key", "w_query",
    "w_query_rope", "w_key_up", "w_value_up", "w_out", "g_ffn", "w_expert_gate",
    "w_expert_up", "w_expert_down", "w_shared_gate", "w_shared_up", "w_shared_down",
)


def local(tokens, latent_cache, rope_cache, lengths, expert_ids, route_weights, *weights):
    named = dict(
        zip(NAMES, (tokens, latent_cache, rope_cache, expert_ids, route_weights) + weights)
    )
    for name in ("g_attn", "g_query", "g_latent", "g_ffn"):
        named[name] = named[name].reshape(1, -1)
    named["rope_cache"] = jnp.swapaxes(rope_cache, 1, 2)
    for name in ("expert_ids", "route_weights", "w_rope_key"):
        named[name] = named[name].T
    ep_size = lax.axis_size("ep")
    tp_size = lax.axis_size("tp")
    devices = ep_size * tp_size
    own = named["w_expert_gate"].shape[0] // tp_size
    rows, width = tokens.shape
    pairs = rows * HEADS
    kvl = latent_cache.shape[2]
    slots = devices * own * CAP

    def holder(name):
        shape = named[name].shape
        if name.startswith("w_expert"):
            shape = (tp_size, own) + shape[1:]
        return pltpu.VMEM(shape, named[name].dtype)

    box = pltpu.VMEM((devices, own * CAP, width), BF16)
    dma = pltpu.SemaphoreType.DMA
    return pl.pallas_call(
        functools.partial(step_kernel, ep_size, tp_size, NAMES),
        out_shape=(
            pltpu.VMEM((rows, width), BF16),
            pltpu.VMEM((rows, kvl + ROPE), BF16),
        ),
        in_specs=[pl.BlockSpec(memory_space=pltpu.SMEM)]
        + [pl.BlockSpec(memory_space=pl.ANY)] * len(NAMES),
        out_specs=(pl.BlockSpec(memory_space=pltpu.VMEM),) * 2,
        scratch_shapes=[holder(name) for name in NAMES]
        + [
            pltpu.VMEM((pairs, kvl), BF16),
            pltpu.VMEM((pairs, ROPE), BF16),
            pltpu.VMEM((pairs, kvl), BF16),
            pltpu.VMEM((slots, rows), BF16),
            pltpu.VMEM((2 * rows, slots), BF16),
            box,
            box,
            box,
            box,
            dma((len(NAMES),)),
            dma((rows // GROUP,)),
            dma((rows // GROUP,)),
            dma((3, tp_size)),
            dma((3, tp_size)),
            dma((devices,)),
            dma((devices,)),
            dma((devices,)),
            dma((devices,)),
            dma((2,)),
        ],
        compiler_params=pltpu.CompilerParams(
            collective_id=0, has_side_effects=True, vmem_limit_bytes=60 * 1024 * 1024
        ),
        name="decode_step",
    )(lengths, *[named[name] for name in NAMES])


def solution(mesh):
    split = ("grp", "ep", "tp")
    in_specs = (
        (P(split, None), P(split, None, None), P(split, None, None), P(split))
        + (P(split, None), P(split, None))
        + (P(),) * 12
        + (P("ep", None, "tp"), P("ep", None, "tp"), P("ep", "tp", None))
        + (P(),) * 3
    )
    out_specs = (P(split, None), P(split, None))
    return jax.shard_map(local, mesh=mesh, in_specs=in_specs, out_specs=out_specs, check_vma=False)
```

profile of v0, /device:TPU:0, one launch (start us, length us, event | category | flops | bytes accessed | tf_op | source)
XLA Modules:
  0.0 24.9 jit_solution(3510821376923344646)
XLA Ops:
  0.6 23.1 %decode_step.1 = (bf16[16,1024]{1,0:T(8,128)(2,1)S(1)}, bf16[16,288]{1,0:T(8,128)(2,1)S(1)}) custom-call(s32[16]{0:T(128)} %lens.1, bf16[16,1024]{1,0:T(8,128)(2,1)} %refs_0_.1, bf16[16,1024,256]{2,1,0:T(8,128)(2,1)} %refs_1_.1, bf16[16,32,1024]{2,1,0:T(8,128)(2,1)} %bitcast.8, s32[4,16]{1,0:T(4,128)} %bitcast.12, f32[4,16]{1,0:T(4,128)} %bitcast.13, ...), custom_call_target="tpu_custom_call" | custom-call | tf_op jit(solution)/shard_map/decode_step/pallas_call | solution.py:382
  23.7 0.6 %copy.28 = bf16[16,1024]{1,0:T(8,128)(2,1)} copy(bf16[16,1024]{1,0:T(8,128)(2,1)S(1)} %get-tuple-element.2) | data formatting | bytes 65536
  24.3 0.6 %copy.29 = bf16[16,288]{1,0:T(8,128)(2,1)} copy(bf16[16,288]{1,0:T(8,128)(2,1)S(1)} %get-tuple-element.3) | data formatting | bytes 18432
where the time goes:
time: 25.1 us; the launch traced here: 24.9 us
  Pallas kernels  23.1 us (92%)
  local copies, waits for them, and re-layouts  1.22 us (5%)
  between operations  0.65 us (3%)
    pallas_call x1, Pallas kernels, local(): pl.pallas_call(functools.partial(step_kernel, ep_size, tp_size, NAMES), o...  23.1 us
    unnamed x2, local copies, waits for them, and re-layouts  1.22 us

commit v1 on v0

--- a/solution.py
+++ b/solution.py
@@ -46,7 +46,7 @@
     return jnp.where(cond, 1.0, 0.0).astype(BF16)
 
 
-def step_kernel(ep_size, tp_size, names, lens, *refs):
+def step_kernel(ep_size, tp_size, names, *refs):
     count = len(names)
     hbm = dict(zip(names, refs[:count]))
     out_ref, entry_ref = refs[count : count + 2]
@@ -57,7 +57,6 @@
         qr_ref,
         mix_ref,
         spread_ref,
-        weight_ref,
         outbox,
         inbox,
         ret_out,
@@ -71,7 +70,6 @@
         out_recv,
         back_send,
         back_recv,
-        own_sem,
     ) = refs[count:]
     rows, width = hbm["tokens"].shape
     length = hbm["latent_cache"].shape[1]
@@ -82,17 +80,34 @@
     ep = lax.axis_index("ep")
     tp = lax.axis_index("tp")
     me = ep * tp_size + tp
+    paired = devices & (devices - 1) == 0
+
+    def flip(d, s):
+        total = 0
+        for k in range(devices.bit_length() - 1):
+            total = total + ((d // (1 << k) + s // (1 << k)) % 2) * (1 << k)
+        return total
+
+    def target(s):
+        return flip(me, s) if paired else lax.rem(me + s, devices)
+
+    def source(s):
+        return flip(me, s) if paired else lax.rem(me + devices - s, devices)
 
     def ident(d):
         return {"ep": d // tp_size, "tp": d % tp_size}
 
-    barrier = pltpu.get_barrier_semaphore()
-
-    @pl.loop(1, devices)
-    def _(i):
-        pl.semaphore_signal(
-            barrier, inc=1, device_id=ident(lax.rem(me + i, devices)), device_id_type=MESH
-        )
+    def each(steps, visit):
+        if len(steps) <= 16:
+            for s in steps:
+                visit(s)
+        else:
+            low = min(steps)
+            high = max(steps)
+
+            @pl.loop(0, high - low + 1)
+            def _(i):
+                visit(high - i)
 
     expert_names = ("w_expert_gate", "w_expert_up", "w_expert_down")
 
@@ -115,15 +130,21 @@
         )
 
     groups = rows // GROUP
-    early = (
-        "expert_ids", "route_weights", "tokens", "g_attn", "g_query", "g_latent", "g_ffn",
-        "w_query_down", "w_latent_down", "w_rope_key", "w_query", "w_query_rope", "w_key_up",
-    )
+    first = ("tokens", "g_attn", "w_query_down", "g_query", "lengths", "expert_ids")
+    second = ("w_query", "w_query_rope", "w_key_up")
     late = (
-        "w_value_up", "w_out", "w_shared_gate", "w_shared_up", "w_shared_down",
+        "w_value_up", "w_out", "g_ffn", "w_shared_gate", "w_shared_up", "w_shared_down",
+        "route_weights", "w_latent_down", "g_latent", "w_rope_key",
     ) + expert_names
-    for name in early:
+    for name in first + second:
         load(name).start()
+    barrier = pltpu.get_barrier_semaphore()
+
+    @pl.loop(1, devices)
+    def _(i):
+        pl.semaphore_signal(
+            barrier, inc=1, device_id=ident(lax.rem(me + i, devices)), device_id_type=MESH
+        )
 
     @pl.loop(0, groups)
     def _(g):
@@ -136,27 +157,24 @@
     def ready(name):
         load(name).wait()
         return vmem[name]
-
-    ids = ready("expert_ids")[...]
-    route = ready("route_weights")[...]
+    for name in first:
+        load(name).wait()
+    lens = vmem["lengths"]
+    ids = vmem["expert_ids"][...]
     slot = iota((slots, rows), 0)
-    slot_expert = lax.shift_right_logical(slot, 2)
+    step = lax.div(slot, block)
+    if paired:
+        owner = lax.bitwise_xor(step, jnp.zeros_like(step) + me)
+    else:
+        owner = lax.rem(step + me, devices)
+    slot_expert = owner * own_experts + lax.div(lax.rem(slot, block), CAP)
     named = jnp.zeros((slots, rows), F32)
-    slot_weight = jnp.zeros((slots, rows), F32)
     for k in range(ids.shape[0]):
-        hit = slot_expert == ids[k : k + 1, :]
-        named = jnp.where(hit, 1.0, named)
-        slot_weight = jnp.where(hit, route[k : k + 1, :], slot_weight)
+        named = jnp.where(slot_expert == ids[k : k + 1, :], 1.0, named)
     before = onehot(iota((rows, rows), 0) < iota((rows, rows), 1))
     rank = nn(named.astype(BF16), before)
     taken = jnp.logical_and(named > 0.5, rank == (slot & (CAP - 1)).astype(F32))
     spread_ref[...] = onehot(taken)
-    slot_weight = jnp.where(taken, slot_weight, 0.0)
-    high = slot_weight.astype(BF16)
-    low = (slot_weight - high.astype(F32)).astype(BF16)
-    eye = onehot(iota((rows, rows), 0) == iota((rows, rows), 1))
-    weight_ref[0:rows, :] = nt(eye, high).astype(BF16)
-    weight_ref[rows : 2 * rows, :] = nt(eye, low).astype(BF16)
 
     row_id = iota((rows, 128), 0)
     position = jnp.zeros((rows, 128), F32)
@@ -170,19 +188,9 @@
     sine = jnp.sin(angle)
     sine = jnp.where((lane & (ROPE - 1)) < half, -sine, sine)
 
-    tokens = ready("tokens")[...].astype(F32)
-    normed = rms(tokens, ready("g_attn")[...]).astype(BF16)
-    gain_query = ready("g_query")[...]
-    query_low = rms(nn(normed, ready("w_query_down")[...]), gain_query).astype(BF16)
-    gain_latent = ready("g_latent")[...]
-    latent_new = rms(nn(normed, ready("w_latent_down")[...]), gain_latent)
-    key = nt(normed, ready("w_rope_key")[...])
-    swapped = jnp.concatenate([key[:, half:], key[:, :half]], axis=1)
-    key_new = key * cosine[:, :ROPE] + swapped * sine[:, :ROPE]
-    kvl = latent_new.shape[1]
-    entry_ref[:, 0:kvl] = latent_new.astype(BF16)
-    entry_ref[:, kvl : kvl + ROPE] = key_new.astype(BF16)
-
+    tokens = vmem["tokens"][...].astype(F32)
+    normed = rms(tokens, vmem["g_attn"][...]).astype(BF16)
+    query_low = rms(nn(normed, vmem["w_query_down"][...]), vmem["g_query"][...]).astype(BF16)
     query = nn(query_low, ready("w_query")[...]).astype(BF16)
     turn = nn(query_low, ready("w_query_rope")[...])
     rope_width = turn.shape[1]
@@ -203,7 +211,6 @@
     def head_mask(columns, shift):
         head = iota((pairs, columns), 0) & (HEADS - 1)
         return head == lax.shift_right_logical(iota((pairs, columns), 1), shift)
-
     nope_mask = head_mask(query.shape[1], 6)
     spread_query = jnp.where(nope_mask, nn(repeat, query), 0.0).astype(BF16)
     ql_ref[...] = nt(spread_query, ready("w_key_up")[...]).astype(BF16)
@@ -231,8 +238,7 @@
     scale = (NOPE + ROPE) ** (-0.5)
     time_lane = iota((HEADS, length), 1)
 
-    @pl.loop(0, groups)
-    def _(g):
+    def attend(g):
         for copy in cache_copies(g):
             copy.wait()
         parts = []
@@ -254,95 +260,99 @@
             mixed = nn(weights, vmem["latent_cache"][s])
             mix_ref[part, :] = (mixed / total).astype(BF16)
 
+    @pl.loop(0, groups - 1)
+    def _(g):
+        attend(g)
+
     pl.semaphore_wait(barrier, devices - 1)
     for copy in swaps:
         copy.start()
 
+    attend(groups - 1)
     heads_all = nn(mix_ref[...], ready("w_value_up")[...])
     heads_all = jnp.where(head_mask(heads_all.shape[1], 6), heads_all, 0.0).astype(BF16)
     gather = onehot(iota((rows, pairs), 0) == lax.shift_right_logical(iota((rows, pairs), 1), 4))
     value_heads = nn(gather, heads_all).astype(BF16)
     hidden = (tokens + nn(value_heads, ready("w_out")[...])).astype(BF16).astype(F32)
     normed_ffn = rms(hidden, ready("g_ffn")[...]).astype(BF16)
-
     box = nn(spread_ref[...], normed_ffn).astype(BF16)
-    for d in range(devices):
-        outbox[d] = box[d * block : (d + 1) * block, :]
-
-    def own_copy(src, dst, i):
-        return pltpu.make_async_copy(src.at[me], dst.at[me], own_sem.at[i])
-
-    def post(src, dst, send, recv, d):
+    for s in range(devices):
+        place = inbox if s == 0 else outbox
+        place[s] = box[s * block : (s + 1) * block, :]
+
+    def message(src, dst, send, recv, s, d):
         return pltpu.make_async_remote_copy(
-            src_ref=src.at[d],
-            dst_ref=dst.at[me],
-            send_sem=send.at[d],
-            recv_sem=recv.at[me],
+            src_ref=src.at[s],
+            dst_ref=dst.at[s],
+            send_sem=send.at[s],
+            recv_sem=recv.at[s],
             device_id=ident(d),
             device_id_type=MESH,
         )
 
-    def arrival(dst, send, recv, d):
-        return pltpu.make_async_remote_copy(
-            src_ref=dst.at[d],
-            dst_ref=dst.at[d],
-            send_sem=send.at[d],
-            recv_sem=recv.at[d],
-            device_id=ident(d),
-            device_id_type=MESH,
-        )
-
-    def send_all(src, dst, send, recv, i):
-        @pl.loop(1, devices)
-        def _(step):
-            post(src, dst, send, recv, lax.rem(me + step, devices)).start()
-
-        own_copy(src, dst, i).start()
-
-    def take_all(src, dst, send, recv, i):
-        own_copy(src, dst, i).wait()
-
-        @pl.loop(1, devices)
-        def _(step):
-            arrival(dst, send, recv, lax.rem(me + step, devices)).wait_recv()
-
-    def drain(src, dst, send, recv):
-        @pl.loop(1, devices)
-        def _(step):
-            post(src, dst, send, recv, lax.rem(me + step, devices)).wait_send()
-
-    send_all(outbox, inbox, out_send, out_recv, 0)
-
+    def there(s):
+        return message(outbox, inbox, out_send, out_recv, s, target(s))
+
+    def back(s):
+        return message(ret_out, ret_in, back_send, back_recv, s, source(s))
+    each(range(devices - 1, 0, -1), lambda s: there(s).start())
     shared_gate = nn(normed_ffn, ready("w_shared_gate")[...])
     shared_up = nn(normed_ffn, ready("w_shared_up")[...])
     shared_hidden = (silu(shared_gate) * shared_up).astype(BF16)
     base = hidden + nn(shared_hidden, ready("w_shared_down")[...])
+    gain_latent = ready("g_latent")[...]
+    latent_new = rms(nn(normed, ready("w_latent_down")[...]), gain_latent)
+    key = nt(normed, ready("w_rope_key")[...])
+    swapped = jnp.concatenate([key[:, half:], key[:, :half]], axis=1)
+    key_new = key * cosine[:, :ROPE] + swapped * sine[:, :ROPE]
+    kvl = latent_new.shape[1]
+    entry_ref[:, 0:kvl] = latent_new.astype(BF16)
+    entry_ref[:, kvl : kvl + ROPE] = key_new.astype(BF16)
+    route = ready("route_weights")[...]
+    slot_weight = jnp.zeros((slots, rows), F32)
+    for k in range(ids.shape[0]):
+        hit = slot_expert == ids[k : k + 1, :]
+        slot_weight = jnp.where(hit, route[k : k + 1, :], slot_weight)
+    slot_weight = jnp.where(spread_ref[...].astype(F32) > 0.5, slot_weight, 0.0)
+    high = slot_weight.astype(BF16)
+    low = (slot_weight - high.astype(F32)).astype(BF16)
+    eye = onehot(iota((rows, rows), 0) == iota((rows, rows), 1))
+    weight_high = nt(eye, high).astype(BF16)
+    weight_low = nt(eye, low).astype(BF16)
     for name in expert_names:
         load(name).wait()
     for copy in swaps:
         copy.wait()
-
-    take_all(outbox, inbox, out_send, out_recv, 0)
-
     gates, ups, downs = (vmem[name] for name in expert_names)
-    for e in range(own_experts):
-        x = jnp.concatenate(
-            [inbox[d, e * CAP : (e + 1) * CAP, :] for d in range(devices)], axis=0
-        )
-        total = jnp.zeros((devices * CAP, width), F32)
-        for t in range(tp_size):
-            unit = (silu(nn(x, gates[t, e])) * nn(x, ups[t, e])).astype(BF16)
-            total = total + nn(unit, downs[t, e]).astype(BF16).astype(F32)
-        total = total.astype(BF16)
-        for d in range(devices):
-            ret_out[d, e * CAP : (e + 1) * CAP, :] = total[d * CAP : (d + 1) * CAP, :]
-    send_all(ret_out, ret_in, back_send, back_recv, 1)
-    drain(outbox, inbox, out_send, out_recv)
-    take_all(ret_out, ret_in, back_send, back_recv, 1)
-    returned = jnp.concatenate([ret_in[d] for d in range(devices)], axis=0)
-    both = nn(weight_ref[...], returned)
-    out_ref[...] = (base + both[0:rows, :] + both[rows : 2 * rows, :]).astype(BF16)
-    drain(ret_out, ret_in, back_send, back_recv)
+
+    def serve(steps):
+        for e in range(own_experts):
+            x = jnp.concatenate(
+                [inbox[s, e * CAP : (e + 1) * CAP, :] for s in steps], axis=0
+            )
+            total = jnp.zeros((len(steps) * CAP, width), F32)
+            for t in range(tp_size):
+                unit = (silu(nn(x, gates[t, e])) * nn(x, ups[t, e])).astype(BF16)
+                total = total + nn(unit, downs[t, e]).astype(BF16).astype(F32)
+            total = total.astype(BF16)
+            for i, s in enumerate(steps):
+                place = ret_in if s == 0 else ret_out
+                place[s, e * CAP : (e + 1) * CAP, :] = total[i * CAP : (i + 1) * CAP, :]
+
+    quarter = max(devices // 4, 1)
+    chunks = [range(i, min(i + quarter, devices)) for i in range(0, devices, quarter)]
+    chunks = chunks[:1] + chunks[:0:-1]
+    for chunk in chunks:
+        remote = range(max(chunk[-1], 0), max(chunk[0], 1) - 1, -1)
+        each(remote, lambda s: there(s).wait_recv())
+        serve(chunk)
+        each(remote, lambda s: back(s).start())
+    each(range(devices - 1, 0, -1), lambda s: there(s).wait_send())
+    each(range(devices - 1, 0, -1), lambda s: back(s).wait_send())
+    each(range(devices - 1, 0, -1), lambda s: back(s).wait_recv())
+    returned = jnp.concatenate([ret_in[s] for s in range(devices)], axis=0)
+    both = nn(weight_high, returned) + nn(weight_low, returned)
+    out_ref[...] = (base + both).astype(BF16)
 
 
 NAMES = (
@@ -350,12 +360,13 @@
     "w_query_down", "g_query", "w_latent_down", "g_latent", "w_rope_key", "w_query",
     "w_query_rope", "w_key_up", "w_value_up", "w_out", "g_ffn", "w_expert_gate",
     "w_expert_up", "w_expert_down", "w_shared_gate", "w_shared_up", "w_shared_down",
+    "lengths",
 )
 
 
 def local(tokens, latent_cache, rope_cache, lengths, expert_ids, route_weights, *weights):
     named = dict(
-        zip(NAMES, (tokens, latent_cache, rope_cache, expert_ids, route_weights) + weights)
+        zip(NAMES, (tokens, latent_cache, rope_cache, expert_ids, route_weights) + weights + (lengths,))
     )
     for name in ("g_attn", "g_query", "g_latent", "g_ffn"):
         named[name] = named[name].reshape(1, -1)
@@ -375,6 +386,8 @@
         shape = named[name].shape
         if name.startswith("w_expert"):
             shape = (tp_size, own) + shape[1:]
+        if name == "lengths":
+            return pltpu.SMEM(shape, named[name].dtype)
         return pltpu.VMEM(shape, named[name].dtype)
 
     box = pltpu.VMEM((devices, own * CAP, width), BF16)
@@ -385,8 +398,7 @@
             pltpu.VMEM((rows, width), BF16),
             pltpu.VMEM((rows, kvl + ROPE), BF16),
         ),
-        in_specs=[pl.BlockSpec(memory_space=pltpu.SMEM)]
-        + [pl.BlockSpec(memory_space=pl.ANY)] * len(NAMES),
+        in_specs=[pl.BlockSpec(memory_space=pl.ANY)] * len(NAMES),
         out_specs=(pl.BlockSpec(memory_space=pltpu.VMEM),) * 2,
         scratch_shapes=[holder(name) for name in NAMES]
         + [
@@ -394,7 +406,6 @@
             pltpu.VMEM((pairs, ROPE), BF16),
             pltpu.VMEM((pairs, kvl), BF16),
             pltpu.VMEM((slots, rows), BF16),
-            pltpu.VMEM((2 * rows, slots), BF16),
             box,
             box,
             box,
@@ -408,13 +419,12 @@
             dma((devices,)),
             dma((devices,)),
             dma((devices,)),
-            dma((2,)),
         ],
         compiler_params=pltpu.CompilerParams(
             collective_id=0, has_side_effects=True, vmem_limit_bytes=60 * 1024 * 1024
         ),
         name="decode_step",
-    )(lengths, *[named[name] for name in NAMES])
+    )(*[named[name] for name in NAMES])
 
 
 def solution(mesh):

time: 25.1 us -> 23.5 us (0.936)
  Pallas kernels: 23.1 us -> 21.5 us
    pallas_call x1, Pallas kernels: 23.1 us -> 21.5 us  [local(): pl.pallas_call(functools.partial(step_kernel, ep_size, tp_size, NAMES), o...]
where the time goes in v1:
time: 23.5 us; the launch traced here: 23.4 us
  Pallas kernels  21.5 us (91%)
  local copies, waits for them, and re-layouts  1.22 us (5%)
  between operations  0.65 us (3%)
    pallas_call x1, Pallas kernels, local(): pl.pallas_call(functools.partial(step_kernel, ep_size, tp_size, NAMES), o...  21.5 us
    unnamed x2, local copies, waits for them, and re-layouts  1.22 us

profile of v1, /device:TPU:0, one launch (start us, length us, event | category | flops | bytes accessed | tf_op | source)
XLA Modules:
  0.0 23.4 jit_solution(8373218444491074421)
XLA Ops:
  0.6 21.5 %decode_step.1 = (bf16[16,1024]{1,0:T(8,128)(2,1)S(1)}, bf16[16,288]{1,0:T(8,128)(2,1)S(1)}) custom-call(bf16[16,1024]{1,0:T(8,128)(2,1)} %refs_0_.1, bf16[16,1024,256]{2,1,0:T(8,128)(2,1)} %refs_1_.1, bf16[16,32,1024]{2,1,0:T(8,128)(2,1)} %bitcast.8, s32[4,16]{1,0:T(4,128)} %bitcast.12, f32[4,16]{1,0:T(4,128)} %bitcast.13, f32[1,1024]{1,0:T(1,128)} %bitcast.10, ...), custom_call_target="tpu_custom_call" | custom-call | tf_op jit(solution)/shard_map/decode_step/pallas_call | solution.py:395
  22.1 0.6 %copy.28 = bf16[16,1024]{1,0:T(8,128)(2,1)} copy(bf16[16,1024]{1,0:T(8,128)(2,1)S(1)} %get-tuple-element.2) | data formatting | bytes 65536
  22.8 0.6 %copy.29 = bf16[16,288]{1,0:T(8,128)(2,1)} copy(bf16[16,288]{1,0:T(8,128)(2,1)S(1)} %get-tuple-element.3) | data formatting | bytes 18432

commit v2 on v1

--- a/solution.py
+++ b/solution.py
@@ -12,7 +12,7 @@
 ROPE = 32
 VDIM = 64
 CAP = 4
-GROUP = 8
+GROUP = 4
 
 norm_eps = 1e-06
 masked_score = -1e30
@@ -56,6 +56,7 @@
         ql_ref,
         qr_ref,
         mix_ref,
+        turned_ref,
         spread_ref,
         outbox,
         inbox,
@@ -73,49 +74,49 @@
     ) = refs[count:]
     rows, width = hbm["tokens"].shape
     length = hbm["latent_cache"].shape[1]
-    own_experts = vmem["w_expert_gate"].shape[1]
+    own_experts = vmem["w_expert_gate"].shape[0]
     devices = ep_size * tp_size
     block = own_experts * CAP
     slots = devices * block
     ep = lax.axis_index("ep")
     tp = lax.axis_index("tp")
     me = ep * tp_size + tp
-    paired = devices & (devices - 1) == 0
-
-    def flip(d, s):
+    planes = 4 if devices % 4 == 0 else 1
+    crew = devices // planes
+    plane = me // crew
+    seat = me % crew
+
+    def across(k):
         total = 0
-        for k in range(devices.bit_length() - 1):
-            total = total + ((d // (1 << k) + s // (1 << k)) % 2) * (1 << k)
+        for b in range(planes.bit_length() - 1):
+            total = total + ((plane // (1 << b) + (k >> b)) % 2) * (1 << b)
         return total
-
-    def target(s):
-        return flip(me, s) if paired else lax.rem(me + s, devices)
-
-    def source(s):
-        return flip(me, s) if paired else lax.rem(me + devices - s, devices)
 
     def ident(d):
         return {"ep": d // tp_size, "tp": d % tp_size}
 
-    def each(steps, visit):
-        if len(steps) <= 16:
-            for s in steps:
-                visit(s)
+    def each(low, high, visit):
+        if high - low <= 16:
+            for i in range(low, high):
+                visit(i)
         else:
-            low = min(steps)
-            high = max(steps)
-
-            @pl.loop(0, high - low + 1)
-            def _(i):
-                visit(high - i)
+            pl.loop(low, high)(visit)
 
     expert_names = ("w_expert_gate", "w_expert_up", "w_expert_down")
+
+    def shard(name, owner):
+        axis = 1 if name == "w_expert_down" else 2
+        units = hbm[name].shape[axis]
+        part = pl.ds(pl.multiple_of(owner * units, units), units)
+        if axis == 1:
+            return vmem[name].at[:, part, :]
+        return vmem[name].at[:, :, part]
 
     def load(name):
         i = names.index(name)
         if name in expert_names:
             src = hbm[name].at[pl.ds(tp * own_experts, own_experts)]
-            return pltpu.make_async_copy(src, vmem[name].at[tp], in_sem.at[i])
+            return pltpu.make_async_copy(src, shard(name, tp), in_sem.at[i])
         return pltpu.make_async_copy(hbm[name], vmem[name], in_sem.at[i])
 
     def cache_copies(g):
@@ -132,12 +133,20 @@
     groups = rows // GROUP
     first = ("tokens", "g_attn", "w_query_down", "g_query", "lengths", "expert_ids")
     second = ("w_query", "w_query_rope", "w_key_up")
+    third = ("w_value_up", "w_out", "g_ffn")
     late = (
-        "w_value_up", "w_out", "g_ffn", "w_shared_gate", "w_shared_up", "w_shared_down",
-        "route_weights", "w_latent_down", "g_latent", "w_rope_key",
+        "w_shared_gate", "w_shared_up", "w_shared_down", "route_weights", "w_latent_down",
+        "g_latent", "w_rope_key",
     ) + expert_names
+
+    def begin(g):
+        if g < groups:
+            for copy in cache_copies(g):
+                copy.start()
+
     for name in first + second:
         load(name).start()
+    begin(0)
     barrier = pltpu.get_barrier_semaphore()
 
     @pl.loop(1, devices)
@@ -146,27 +155,17 @@
             barrier, inc=1, device_id=ident(lax.rem(me + i, devices)), device_id_type=MESH
         )
 
-    @pl.loop(0, groups)
-    def _(g):
-        for copy in cache_copies(g):
-            copy.start()
-
-    for name in late:
-        load(name).start()
-
     def ready(name):
         load(name).wait()
         return vmem[name]
     for name in first:
         load(name).wait()
+    begin(1)
     lens = vmem["lengths"]
     ids = vmem["expert_ids"][...]
     slot = iota((slots, rows), 0)
     step = lax.div(slot, block)
-    if paired:
-        owner = lax.bitwise_xor(step, jnp.zeros_like(step) + me)
-    else:
-        owner = lax.rem(step + me, devices)
+    owner = lax.div(step, crew) * crew + lax.rem(lax.rem(step, crew) + seat, crew)
     slot_expert = owner * own_experts + lax.div(lax.rem(slot, block), CAP)
     named = jnp.zeros((slots, rows), F32)
     for k in range(ids.shape[0]):
@@ -191,7 +190,8 @@
     tokens = vmem["tokens"][...].astype(F32)
     normed = rms(tokens, vmem["g_attn"][...]).astype(BF16)
     query_low = rms(nn(normed, vmem["w_query_down"][...]), vmem["g_query"][...]).astype(BF16)
-    query = nn(query_low, ready("w_query")[...]).astype(BF16)
+    begin(2)
+    query = nn(query_low, ready("w_query")[...])
     turn = nn(query_low, ready("w_query_rope")[...])
     rope_width = turn.shape[1]
     rope_lane = iota((rows, rope_width), 1)
@@ -204,21 +204,46 @@
     turned = (
         turn * jnp.concatenate([cosine] * tiles, axis=1)
         + swapped * jnp.concatenate([sine] * tiles, axis=1)
-    ).astype(BF16)
-    pairs = rows * HEADS
-    repeat = onehot(lax.shift_right_logical(iota((pairs, rows), 0), 4) == iota((pairs, rows), 1))
-
-    def head_mask(columns, shift):
-        head = iota((pairs, columns), 0) & (HEADS - 1)
-        return head == lax.shift_right_logical(iota((pairs, columns), 1), shift)
-    nope_mask = head_mask(query.shape[1], 6)
-    spread_query = jnp.where(nope_mask, nn(repeat, query), 0.0).astype(BF16)
-    ql_ref[...] = nt(spread_query, ready("w_key_up")[...]).astype(BF16)
-    spread_turn = jnp.where(head_mask(rope_width, 5), nn(repeat, turned), 0.0).astype(BF16)
-    fold = onehot(
-        (iota((rope_width, ROPE), 0) & (ROPE - 1)) == iota((rope_width, ROPE), 1)
     )
-    qr_ref[...] = nn(spread_turn, fold).astype(BF16)
+    for h in range(HEADS):
+        tile, place = divmod(h * ROPE, 128)
+        lanes = turned[:, tile * 128 : (tile + 1) * 128]
+        if place:
+            lanes = pltpu.roll(lanes, 128 - place, 1)
+        qr_ref[h * rows : (h + 1) * rows, :] = lanes
+    def put_wide(ref, part, value):
+        for t in range(ref.shape[0]):
+            ref[t, part, :] = value[:, t * 128 : (t + 1) * 128]
+
+    def get_wide(ref, part):
+        return jnp.concatenate([ref[t, part, :] for t in range(ref.shape[0])], axis=1)
+
+    span = 256
+    quad = span // NOPE
+    quad_lane = iota((rows, span), 1) // NOPE
+    w_key_up = ready("w_key_up")
+    for g in range(3, groups):
+        begin(g)
+    for copy in cache_copies(0):
+        copy.wait()
+
+    def turn_keys(s):
+        turned_ref[s % (2 * GROUP)] = vmem["latent_cache"][s].T
+
+    for name in third:
+        load(name).start()
+    for s in range(GROUP):
+        turn_keys(s)
+    for n in range(HEADS // quad):
+        piece = query[:, n * span : (n + 1) * span]
+        spread_query = jnp.concatenate(
+            [jnp.where(quad_lane == j, piece, 0.0) for j in range(quad)], axis=0
+        )
+        put_wide(
+            ql_ref,
+            pl.ds(n * quad * rows, quad * rows),
+            nt(spread_query.astype(BF16), w_key_up[:, n * span : (n + 1) * span]),
+        )
 
     swaps = []
     for p in range(1, tp_size):
@@ -227,7 +252,7 @@
             swaps.append(
                 pltpu.make_async_remote_copy(
                     src_ref=hbm[name].at[pl.ds(peer * own_experts, own_experts)],
-                    dst_ref=vmem[name].at[tp],
+                    dst_ref=shard(name, tp),
                     send_sem=swap_send.at[i, p],
                     recv_sem=swap_recv.at[i, p],
                     device_id={"tp": peer},
@@ -238,64 +263,100 @@
     scale = (NOPE + ROPE) ** (-0.5)
     time_lane = iota((HEADS, length), 1)
 
-    def attend(g):
-        for copy in cache_copies(g):
-            copy.wait()
-        parts = []
-        scored = []
-        for j in range(GROUP):
-            s = g * GROUP + j
-            part = pl.ds(pl.multiple_of(s * HEADS, HEADS), HEADS)
-            parts.append((s, part))
-            scores = nt(ql_ref[part, :], vmem["latent_cache"][s])
-            scored.append(scores + nn(qr_ref[part, :], vmem["rope_cache"][s]))
+    def head_rows(s):
+        return pl.ds(s, HEADS, stride=rows)
+
+    def score(s):
+        query_latent = get_wide(ql_ref, head_rows(s)).astype(BF16)
+        query_rope = qr_ref[head_rows(s), :][:, 0:ROPE].astype(BF16)
+        found = nn(query_latent, turned_ref[s % (2 * GROUP)])
+        return found + nn(query_rope, vmem["rope_cache"][s])
+
+    def soften(s, scores):
+        live = time_lane < lens[s]
+        scores = jnp.where(live, scores * scale, masked_score)
+        top = jnp.max(scores, axis=1, keepdims=True)
+        weights = jnp.where(live, jnp.exp(scores - top), 0.0)
+        return weights.astype(BF16), jnp.sum(weights, axis=1, keepdims=True)
+
+    def mix(s, weights, total):
+        mixed = nn(weights, vmem["latent_cache"][s])
+        put_wide(mix_ref, head_rows(s), mixed / total)
+
+    members = [range(g * GROUP, (g + 1) * GROUP) for g in range(groups)]
+    scored = []
+    for g in range(groups + 1):
+        if g + 1 < groups:
+            for copy in cache_copies(g + 1):
+                copy.wait()
+        if g == 0:
+            for name in late:
+                load(name).start()
+        if g == groups - 1:
+            pl.semaphore_wait(barrier, devices - 1)
+            for copy in swaps:
+                copy.start()
+        if g == groups:
+            for name in third:
+                load(name).wait()
         soft = []
-        for (s, part), scores in zip(parts, scored):
-            live = time_lane < lens[s]
-            scores = jnp.where(live, scores * scale, masked_score)
-            top = jnp.max(scores, axis=1, keepdims=True)
-            weights = jnp.where(live, jnp.exp(scores - top), 0.0)
-            soft.append((weights.astype(BF16), jnp.sum(weights, axis=1, keepdims=True)))
-        for (s, part), (weights, total) in zip(parts, soft):
-            mixed = nn(weights, vmem["latent_cache"][s])
-            mix_ref[part, :] = (mixed / total).astype(BF16)
-
-    @pl.loop(0, groups - 1)
-    def _(g):
-        attend(g)
-
-    pl.semaphore_wait(barrier, devices - 1)
-    for copy in swaps:
-        copy.start()
-
-    attend(groups - 1)
-    heads_all = nn(mix_ref[...], ready("w_value_up")[...])
-    heads_all = jnp.where(head_mask(heads_all.shape[1], 6), heads_all, 0.0).astype(BF16)
-    gather = onehot(iota((rows, pairs), 0) == lax.shift_right_logical(iota((rows, pairs), 1), 4))
-    value_heads = nn(gather, heads_all).astype(BF16)
-    hidden = (tokens + nn(value_heads, ready("w_out")[...])).astype(BF16).astype(F32)
-    normed_ffn = rms(hidden, ready("g_ffn")[...]).astype(BF16)
+        if g > 0:
+            soft = [soften(s, scores) for s, scores in zip(members[g - 1], scored)]
+        if g < groups:
+            scored = [score(s) for s in members[g]]
+        if g + 1 < groups:
+            for s in members[g + 1]:
+                turn_keys(s)
+        for s, (weights, total) in zip(members[g - 1], soft):
+            mix(s, weights, total)
+    value_pieces = []
+    for n in range(HEADS // quad):
+        part = get_wide(mix_ref, pl.ds(n * quad * rows, quad * rows)).astype(BF16)
+        part = nn(part, vmem["w_value_up"][:, n * span : (n + 1) * span])
+        piece = part[0:rows]
+        for j in range(1, quad):
+            piece = jnp.where(quad_lane == j, part[j * rows : (j + 1) * rows], piece)
+        value_pieces.append(piece.astype(BF16))
+    value_heads = jnp.concatenate(value_pieces, axis=1)
+    hidden = (tokens + nn(value_heads, vmem["w_out"][...])).astype(BF16).astype(F32)
+    normed_ffn = rms(hidden, vmem["g_ffn"][...]).astype(BF16)
     box = nn(spread_ref[...], normed_ffn).astype(BF16)
     for s in range(devices):
-        place = inbox if s == 0 else outbox
-        place[s] = box[s * block : (s + 1) * block, :]
-
-    def message(src, dst, send, recv, s, d):
+        outbox[s] = box[s * block : (s + 1) * block, :]
+    inbox[plane * crew] = outbox[plane * crew]
+
+    def message(src, dst, send, recv, p, i, d):
         return pltpu.make_async_remote_copy(
-            src_ref=src.at[s],
-            dst_ref=dst.at[s],
-            send_sem=send.at[s],
-            recv_sem=recv.at[s],
-            device_id=ident(d),
+            src_ref=src.at[p * crew + i],
+            dst_ref=dst.at[plane * crew + i],
+            send_sem=send.at[p * crew + i],
+            recv_sem=recv.at[plane * crew + i],
+            device_id=ident(p * crew + d),
             device_id_type=MESH,
         )
 
-    def there(s):
-        return message(outbox, inbox, out_send, out_recv, s, target(s))
-
-    def back(s):
-        return message(ret_out, ret_in, back_send, back_recv, s, source(s))
-    each(range(devices - 1, 0, -1), lambda s: there(s).start())
+    def there(p, i):
+        return message(outbox, inbox, out_send, out_recv, p, i, lax.rem(seat + i, crew))
+
+    def back(p, i):
+        return message(ret_out, ret_in, back_send, back_recv, p, i, lax.rem(seat + crew - i, crew))
+
+    def arrival(dst, recv, p, i):
+        spot = dst.at[p * crew + i]
+        return pltpu.make_async_remote_copy(
+            src_ref=spot,
+            dst_ref=spot,
+            send_sem=out_send.at[p * crew + i],
+            recv_sem=recv.at[p * crew + i],
+            device_id=ident(me),
+            device_id_type=MESH,
+        )
+
+    def peers(visit):
+        for k in range(planes - 1, -1, -1):
+            p = across(k)
+            each(0 if k else 1, crew, lambda i, p=p: visit(p, i))
+    peers(lambda p, i: there(p, i).start())
     shared_gate = nn(normed_ffn, ready("w_shared_gate")[...])
     shared_up = nn(normed_ffn, ready("w_shared_up")[...])
     shared_hidden = (silu(shared_gate) * shared_up).astype(BF16)
@@ -325,31 +386,34 @@
         copy.wait()
     gates, ups, downs = (vmem[name] for name in expert_names)
 
-    def serve(steps):
+    def serve(p):
+        steps = range(p * crew, (p + 1) * crew)
         for e in range(own_experts):
             x = jnp.concatenate(
                 [inbox[s, e * CAP : (e + 1) * CAP, :] for s in steps], axis=0
             )
-            total = jnp.zeros((len(steps) * CAP, width), F32)
-            for t in range(tp_size):
-                unit = (silu(nn(x, gates[t, e])) * nn(x, ups[t, e])).astype(BF16)
-                total = total + nn(unit, downs[t, e]).astype(BF16).astype(F32)
-            total = total.astype(BF16)
+            unit = (silu(nn(x, gates[e])) * nn(x, ups[e])).astype(BF16)
+            total = nn(unit, downs[e]).astype(BF16)
             for i, s in enumerate(steps):
-                place = ret_in if s == 0 else ret_out
-                place[s, e * CAP : (e + 1) * CAP, :] = total[i * CAP : (i + 1) * CAP, :]
-
-    quarter = max(devices // 4, 1)
-    chunks = [range(i, min(i + quarter, devices)) for i in range(0, devices, quarter)]
-    chunks = chunks[:1] + chunks[:0:-1]
-    for chunk in chunks:
-        remote = range(max(chunk[-1], 0), max(chunk[0], 1) - 1, -1)
-        each(remote, lambda s: there(s).wait_recv())
-        serve(chunk)
-        each(remote, lambda s: back(s).start())
-    each(range(devices - 1, 0, -1), lambda s: there(s).wait_send())
-    each(range(devices - 1, 0, -1), lambda s: back(s).wait_send())
-    each(range(devices - 1, 0, -1), lambda s: back(s).wait_recv())
+                ret_out[s, e * CAP : (e + 1) * CAP, :] = total[i * CAP : (i + 1) * CAP, :]
+
+    for p in range(planes):
+        each(1, crew, lambda i: arrival(inbox, out_recv, p, i).wait_recv())
+
+        @pl.when(plane != p)
+        def _():
+            arrival(inbox, out_recv, p, 0).wait_recv()
+        serve(p)
+        each(1, crew, lambda i: back(p, i).start())
+
+        @pl.when(plane != p)
+        def _():
+            back(p, 0).start()
+
+    ret_in[plane * crew] = ret_out[plane * crew]
+    peers(lambda p, i: there(p, i).wait_send())
+    peers(lambda p, i: back(p, i).wait_send())
+    peers(lambda p, i: arrival(ret_in, back_recv, p, i).wait_recv())
     returned = jnp.concatenate([ret_in[s] for s in range(devices)], axis=0)
     both = nn(weight_high, returned) + nn(weight_low, returned)
     out_ref[...] = (base + both).astype(BF16)
@@ -379,13 +443,16 @@
     own = named["w_expert_gate"].shape[0] // tp_size
     rows, width = tokens.shape
     pairs = rows * HEADS
-    kvl = latent_cache.shape[2]
+    length, kvl = latent_cache.shape[1:]
     slots = devices * own * CAP
 
     def holder(name):
         shape = named[name].shape
         if name.startswith("w_expert"):
-            shape = (tp_size, own) + shape[1:]
+            axis = 1 if name == "w_expert_down" else 2
+            shape = (own,) + tuple(
+                n * tp_size if i == axis else n for i, n in enumerate(shape) if i
+            )
         if name == "lengths":
             return pltpu.SMEM(shape, named[name].dtype)
         return pltpu.VMEM(shape, named[name].dtype)
@@ -402,9 +469,10 @@
         out_specs=(pl.BlockSpec(memory_space=pltpu.VMEM),) * 2,
         scratch_shapes=[holder(name) for name in NAMES]
         + [
-            pltpu.VMEM((pairs, kvl), BF16),
-            pltpu.VMEM((pairs, ROPE), BF16),
-            pltpu.VMEM((pairs, kvl), BF16),
+            pltpu.VMEM((kvl // 128, pairs, 128), F32),
+            pltpu.VMEM((pairs, 128), F32),
+            pltpu.VMEM((kvl // 128, pairs, 128), F32),
+            pltpu.VMEM((2 * GROUP, kvl, length), BF16),
             pltpu.VMEM((slots, rows), BF16),
             box,
             box,

time: 23.5 us -> 21.8 us (0.928)
  Pallas kernels: 21.5 us -> 19.8 us
    pallas_call x1, Pallas kernels: 21.5 us -> 19.8 us  [local(): pl.pallas_call(functools.partial(step_kernel, ep_size, tp_size, NAMES), o...]
where the time goes in v2:
time: 21.8 us; the launch traced here: 21.6 us
  Pallas kernels  19.8 us (91%)
  local copies, waits for them, and re-layouts  1.22 us (6%)
  between operations  0.65 us (3%)
    pallas_call x1, Pallas kernels, local(): pl.pallas_call(functools.partial(step_kernel, ep_size, tp_size, NAMES), o...  19.8 us
    unnamed x2, local copies, waits for them, and re-layouts  1.22 us

profile of v2, /device:TPU:0, one launch (start us, length us, event | category | flops | bytes accessed | tf_op | source)
XLA Modules:
  0.0 21.6 jit_solution(8803678481981401467)
XLA Ops:
  0.6 19.8 %decode_step.1 = (bf16[16,1024]{1,0:T(8,128)(2,1)S(1)}, bf16[16,288]{1,0:T(8,128)(2,1)S(1)}) custom-call(bf16[16,1024]{1,0:T(8,128)(2,1)} %refs_0_.1, bf16[16,1024,256]{2,1,0:T(8,128)(2,1)} %refs_1_.1, bf16[16,32,1024]{2,1,0:T(8,128)(2,1)} %bitcast.8, s32[4,16]{1,0:T(4,128)} %bitcast.12, f32[4,16]{1,0:T(4,128)} %bitcast.13, f32[1,1024]{1,0:T(1,128)} %bitcast.10, ...), custom_call_target="tpu_custom_call" | custom-call | tf_op jit(solution)/shard_map/decode_step/pallas_call | solution.py:462
  20.4 0.6 %copy.28 = bf16[16,1024]{1,0:T(8,128)(2,1)} copy(bf16[16,1024]{1,0:T(8,128)(2,1)S(1)} %get-tuple-element.2) | data formatting | bytes 65536
  21.0 0.6 %copy.29 = bf16[16,288]{1,0:T(8,128)(2,1)} copy(bf16[16,288]{1,0:T(8,128)(2,1)S(1)} %get-tuple-element.3) | data formatting | bytes 18432

commit v3 on v2

--- a/solution.py
+++ b/solution.py
@@ -1,4 +1,5 @@
 import functools
+import math
 
 import jax
 import jax.numpy as jnp
@@ -62,14 +63,13 @@
         inbox,
         ret_out,
         ret_in,
-        in_sem,
+        small_sem,
+        load_sem,
         cache_sem,
-        rope_sem,
         swap_send,
         swap_recv,
-        out_send,
+        send_sem,
         out_recv,
-        back_send,
         back_recv,
     ) = refs[count:]
     rows, width = hbm["tokens"].shape
@@ -112,12 +112,49 @@
             return vmem[name].at[:, part, :]
         return vmem[name].at[:, :, part]
 
-    def load(name):
-        i = names.index(name)
+    small = (
+        "lengths", "expert_ids", "route_weights", "g_attn", "g_query", "g_latent", "g_ffn",
+    )
+    first = ("tokens", "w_query_down")
+    second = ("w_query", "w_query_rope", "w_key_up")
+    third = ("w_value_up", "w_out")
+    fourth = (
+        "w_shared_gate", "w_shared_up", "w_shared_down", "w_latent_down", "w_rope_key",
+    )
+    batches = (first, second, third, fourth, expert_names)
+
+    def source_of(name):
         if name in expert_names:
-            src = hbm[name].at[pl.ds(tp * own_experts, own_experts)]
-            return pltpu.make_async_copy(src, shard(name, tp), in_sem.at[i])
-        return pltpu.make_async_copy(hbm[name], vmem[name], in_sem.at[i])
+            return hbm[name].at[pl.ds(tp * own_experts, own_experts)]
+        return hbm[name]
+
+    def load(batch):
+        if batch in small:
+            sem = small_sem.at[small.index(batch)]
+            return pltpu.make_async_copy(hbm[batch], vmem[batch], sem)
+        sem = load_sem.at[batches.index(batch)]
+        for name in batch:
+            place = shard(name, tp) if name in expert_names else vmem[name]
+            pltpu.make_async_copy(source_of(name), place, sem).start()
+
+    def size_of(ref):
+        return math.prod(ref.shape) * jnp.dtype(ref.dtype).itemsize
+
+    def landed(total, sem):
+        cache = hbm["latent_cache"]
+        row = cache.shape[2] * 2
+        shapes = [
+            (n, total // (n * row))
+            for n in range(1, rows + 1)
+            if total % (16 * n * row) == 0 and total // (n * row) <= length
+        ]
+        n, depth = shapes[0]
+        part = (pl.ds(0, n), pl.ds(0, depth))
+        pltpu.make_async_copy(cache.at[part], vmem["latent_cache"].at[part], sem).wait()
+
+    def finish(batch):
+        total = sum(size_of(source_of(name)) for name in batch)
+        landed(total, load_sem.at[batches.index(batch)])
 
     def cache_copies(g):
         part = pl.ds(g * GROUP, GROUP)
@@ -126,27 +163,24 @@
                 hbm["latent_cache"].at[part], vmem["latent_cache"].at[part], cache_sem.at[g]
             ),
             pltpu.make_async_copy(
-                hbm["rope_cache"].at[part], vmem["rope_cache"].at[part], rope_sem.at[g]
+                hbm["rope_cache"].at[part], vmem["rope_cache"].at[part], cache_sem.at[g]
             ),
         )
 
+    def cache_wait(g):
+        part = pl.ds(0, GROUP)
+        total = size_of(hbm["latent_cache"].at[part]) + size_of(hbm["rope_cache"].at[part])
+        landed(total, cache_sem.at[g])
+
     groups = rows // GROUP
-    first = ("tokens", "g_attn", "w_query_down", "g_query", "lengths", "expert_ids")
-    second = ("w_query", "w_query_rope", "w_key_up")
-    third = ("w_value_up", "w_out", "g_ffn")
-    late = (
-        "w_shared_gate", "w_shared_up", "w_shared_down", "route_weights", "w_latent_down",
-        "g_latent", "w_rope_key",
-    ) + expert_names
-
     def begin(g):
         if g < groups:
             for copy in cache_copies(g):
                 copy.start()
 
-    for name in first + second:
+    load(first)
+    for name in small:
         load(name).start()
-    begin(0)
     barrier = pltpu.get_barrier_semaphore()
 
     @pl.loop(1, devices)
@@ -155,11 +189,11 @@
             barrier, inc=1, device_id=ident(lax.rem(me + i, devices)), device_id_type=MESH
         )
 
-    def ready(name):
+    load(second)
+    begin(0)
+    for name in small:
         load(name).wait()
-        return vmem[name]
-    for name in first:
-        load(name).wait()
+    finish(first)
     begin(1)
     lens = vmem["lengths"]
     ids = vmem["expert_ids"][...]
@@ -191,8 +225,9 @@
     normed = rms(tokens, vmem["g_attn"][...]).astype(BF16)
     query_low = rms(nn(normed, vmem["w_query_down"][...]), vmem["g_query"][...]).astype(BF16)
     begin(2)
-    query = nn(query_low, ready("w_query")[...])
-    turn = nn(query_low, ready("w_query_rope")[...])
+    finish(second)
+    query = nn(query_low, vmem["w_query"][...])
+    turn = nn(query_low, vmem["w_query_rope"][...])
     rope_width = turn.shape[1]
     rope_lane = iota((rows, rope_width), 1)
     swapped = jnp.where(
@@ -221,17 +256,15 @@
     span = 256
     quad = span // NOPE
     quad_lane = iota((rows, span), 1) // NOPE
-    w_key_up = ready("w_key_up")
+    w_key_up = vmem["w_key_up"]
     for g in range(3, groups):
         begin(g)
-    for copy in cache_copies(0):
-        copy.wait()
+    cache_wait(0)
 
     def turn_keys(s):
         turned_ref[s % (2 * GROUP)] = vmem["latent_cache"][s].T
 
-    for name in third:
-        load(name).start()
+    load(third)
     for s in range(GROUP):
         turn_keys(s)
     for n in range(HEADS // quad):
@@ -253,8 +286,8 @@
                 pltpu.make_async_remote_copy(
                     src_ref=hbm[name].at[pl.ds(peer * own_experts, own_experts)],
                     dst_ref=shard(name, tp),
-                    send_sem=swap_send.at[i, p],
-                    recv_sem=swap_recv.at[i, p],
+                    send_sem=swap_send.at[i, p - 1],
+                    recv_sem=swap_recv.at[i, p - 1],
                     device_id={"tp": peer},
                     device_id_type=MESH,
                 )
@@ -287,18 +320,16 @@
     scored = []
     for g in range(groups + 1):
         if g + 1 < groups:
-            for copy in cache_copies(g + 1):
-                copy.wait()
+            cache_wait(g + 1)
         if g == 0:
-            for name in late:
-                load(name).start()
-        if g == groups - 1:
+            load(fourth)
+            load(expert_names)
+        if g == max(groups - 2, 0):
             pl.semaphore_wait(barrier, devices - 1)
             for copy in swaps:
                 copy.start()
-        if g == groups:
-            for name in third:
-                load(name).wait()
+        if g == max(groups - 1, 0):
+            finish(third)
         soft = []
         if g > 0:
             soft = [soften(s, scores) for s, scores in zip(members[g - 1], scored)]
@@ -325,29 +356,34 @@
         outbox[s] = box[s * block : (s + 1) * block, :]
     inbox[plane * crew] = outbox[plane * crew]
 
-    def message(src, dst, send, recv, p, i, d):
+    def message(src, dst, way, recv, p, i, d):
         return pltpu.make_async_remote_copy(
             src_ref=src.at[p * crew + i],
             dst_ref=dst.at[plane * crew + i],
-            send_sem=send.at[p * crew + i],
-            recv_sem=recv.at[plane * crew + i],
+            send_sem=send_sem.at[way],
+            recv_sem=recv,
             device_id=ident(p * crew + d),
             device_id_type=MESH,
         )
 
+    def gate_of(p, i):
+        return out_recv.at[2 * p] if isinstance(i, int) and i == 0 else out_recv.at[2 * p + 1]
+
     def there(p, i):
-        return message(outbox, inbox, out_send, out_recv, p, i, lax.rem(seat + i, crew))
+        d = lax.rem(seat + i, crew)
+        return message(outbox, inbox, 0, gate_of(plane, i), p, i, d)
 
     def back(p, i):
-        return message(ret_out, ret_in, back_send, back_recv, p, i, lax.rem(seat + crew - i, crew))
-
-    def arrival(dst, recv, p, i):
-        spot = dst.at[p * crew + i]
+        d = lax.rem(seat + crew - i, crew)
+        return message(ret_out, ret_in, 1, back_recv.at[0], p, i, d)
+
+    def bulk(ref, low, size, send, recv):
+        part = ref.at[pl.ds(low, size)]
         return pltpu.make_async_remote_copy(
-            src_ref=spot,
-            dst_ref=spot,
-            send_sem=out_send.at[p * crew + i],
-            recv_sem=recv.at[p * crew + i],
+            src_ref=part,
+            dst_ref=part,
+            send_sem=send,
+            recv_sem=recv,
             device_id=ident(me),
             device_id_type=MESH,
         )
@@ -355,21 +391,23 @@
     def peers(visit):
         for k in range(planes - 1, -1, -1):
             p = across(k)
-            each(0 if k else 1, crew, lambda i, p=p: visit(p, i))
+            if k:
+                visit(p, 0)
+            each(1, crew, lambda i, p=p: visit(p, i))
     peers(lambda p, i: there(p, i).start())
-    shared_gate = nn(normed_ffn, ready("w_shared_gate")[...])
-    shared_up = nn(normed_ffn, ready("w_shared_up")[...])
+    finish(fourth)
+    shared_gate = nn(normed_ffn, vmem["w_shared_gate"][...])
+    shared_up = nn(normed_ffn, vmem["w_shared_up"][...])
     shared_hidden = (silu(shared_gate) * shared_up).astype(BF16)
-    base = hidden + nn(shared_hidden, ready("w_shared_down")[...])
-    gain_latent = ready("g_latent")[...]
-    latent_new = rms(nn(normed, ready("w_latent_down")[...]), gain_latent)
-    key = nt(normed, ready("w_rope_key")[...])
+    base = hidden + nn(shared_hidden, vmem["w_shared_down"][...])
+    latent_new = rms(nn(normed, vmem["w_latent_down"][...]), vmem["g_latent"][...])
+    key = nt(normed, vmem["w_rope_key"][...])
     swapped = jnp.concatenate([key[:, half:], key[:, :half]], axis=1)
     key_new = key * cosine[:, :ROPE] + swapped * sine[:, :ROPE]
     kvl = latent_new.shape[1]
     entry_ref[:, 0:kvl] = latent_new.astype(BF16)
     entry_ref[:, kvl : kvl + ROPE] = key_new.astype(BF16)
-    route = ready("route_weights")[...]
+    route = vmem["route_weights"][...]
     slot_weight = jnp.zeros((slots, rows), F32)
     for k in range(ids.shape[0]):
         hit = slot_expert == ids[k : k + 1, :]
@@ -380,8 +418,7 @@
     eye = onehot(iota((rows, rows), 0) == iota((rows, rows), 1))
     weight_high = nt(eye, high).astype(BF16)
     weight_low = nt(eye, low).astype(BF16)
-    for name in expert_names:
-        load(name).wait()
+    finish(expert_names)
     for copy in swaps:
         copy.wait()
     gates, ups, downs = (vmem[name] for name in expert_names)
@@ -398,11 +435,13 @@
                 ret_out[s, e * CAP : (e + 1) * CAP, :] = total[i * CAP : (i + 1) * CAP, :]
 
     for p in range(planes):
-        each(1, crew, lambda i: arrival(inbox, out_recv, p, i).wait_recv())
+        if crew > 1:
+            gate = out_recv.at[2 * p + 1]
+            bulk(inbox, p * crew + 1, crew - 1, send_sem.at[0], gate).wait_recv()
 
         @pl.when(plane != p)
         def _():
-            arrival(inbox, out_recv, p, 0).wait_recv()
+            bulk(inbox, p * crew, 1, send_sem.at[0], out_recv.at[2 * p]).wait_recv()
         serve(p)
         each(1, crew, lambda i: back(p, i).start())
 
@@ -411,12 +450,24 @@
             back(p, 0).start()
 
     ret_in[plane * crew] = ret_out[plane * crew]
-    peers(lambda p, i: there(p, i).wait_send())
-    peers(lambda p, i: back(p, i).wait_send())
-    peers(lambda p, i: arrival(ret_in, back_recv, p, i).wait_recv())
+    remote = devices - 1
+    bulk(ret_in, 0, remote, send_sem.at[1], back_recv.at[0]).wait_recv()
     returned = jnp.concatenate([ret_in[s] for s in range(devices)], axis=0)
     both = nn(weight_high, returned) + nn(weight_low, returned)
     out_ref[...] = (base + both).astype(BF16)
+    bulk(outbox, 0, remote, send_sem.at[0], back_recv.at[0]).wait_send()
+    bulk(ret_out, 0, remote, send_sem.at[1], back_recv.at[0]).wait_send()
+
+
+def store_kernel(mixed_ref, entry_ref, out_ref, new_ref, sem):
+    copies = (
+        pltpu.make_async_copy(mixed_ref, out_ref, sem.at[0]),
+        pltpu.make_async_copy(entry_ref, new_ref, sem.at[1]),
+    )
+    for copy in copies:
+        copy.start()
+    for copy in copies:
+        copy.wait()
 
 
 NAMES = (
@@ -459,7 +510,7 @@
 
     box = pltpu.VMEM((devices, own * CAP, width), BF16)
     dma = pltpu.SemaphoreType.DMA
-    return pl.pallas_call(
+    mixed, entry = pl.pallas_call(
         functools.partial(step_kernel, ep_size, tp_size, NAMES),
         out_shape=(
             pltpu.VMEM((rows, width), BF16),
@@ -478,21 +529,34 @@
             box,
             box,
             box,
-            dma((len(NAMES),)),
+            dma((7,)),
+            dma((5,)),
             dma((rows // GROUP,)),
-            dma((rows // GROUP,)),
-            dma((3, tp_size)),
-            dma((3, tp_size)),
-            dma((devices,)),
-            dma((devices,)),
-            dma((devices,)),
-            dma((devices,)),
+            dma((3, max(tp_size - 1, 1))),
+            dma((3, max(tp_size - 1, 1))),
+            dma((2,)),
+            dma((2 * (4 if devices % 4 == 0 else 1),)),
+            dma((1,)),
         ],
         compiler_params=pltpu.CompilerParams(
             collective_id=0, has_side_effects=True, vmem_limit_bytes=60 * 1024 * 1024
         ),
         name="decode_step",
     )(*[named[name] for name in NAMES])
+    return pl.pallas_call(
+        store_kernel,
+        out_shape=(
+            jax.ShapeDtypeStruct(mixed.shape, BF16),
+            jax.ShapeDtypeStruct(entry.shape, BF16),
+        ),
+        in_specs=[pl.BlockSpec(memory_space=pltpu.VMEM)] * 2,
+        out_specs=(pl.BlockSpec(memory_space=pl.ANY),) * 2,
+        scratch_shapes=[dma((2,))],
+        name="store_step",
+    )(
+        pltpu.with_memory_space_constraint(mixed, pltpu.VMEM),
+        pltpu.with_memory_space_constraint(entry, pltpu.VMEM),
+    )
 
 
 def solution(mesh):

time: 21.8 us -> 20.3 us (0.931)
  local copies, waits for them, and re-layouts: 1.22 us -> 0 us
  Pallas kernels: 19.8 us -> 19.5 us
    unnamed x2 -> x0, local copies, waits for them, and re-layouts: 1.22 us -> none
    pallas_call x1, Pallas kernels: 19.8 us -> 18.9 us  [local(): pl.pallas_call(functools.partial(step_kernel, ep_size, tp_size, NAMES), o...]
    pallas_call x0 -> x1, Pallas kernels: none -> 0.64 us  [local(): pl.pallas_call(store_kernel, out_shape=(jax.ShapeDtypeStruct(mixed.shape,...]
where the time goes in v3:
time: 20.3 us; the launch traced here: 20.2 us
  Pallas kernels  19.5 us (96%)
  between operations  0.65 us (3%)
    pallas_call x1, Pallas kernels, local(): pl.pallas_call(functools.partial(step_kernel, ep_size, tp_size, NAMES), o...  18.9 us
    pallas_call x1, Pallas kernels, local(): pl.pallas_call(store_kernel, out_shape=(jax.ShapeDtypeStruct(mixed.shape,...  0.64 us

profile of v3, /device:TPU:0, one launch (start us, length us, event | category | flops | bytes accessed | tf_op | source)
XLA Modules:
  0.0 20.2 jit_solution(1625104655307023220)
XLA Ops:
  0.6 18.9 %decode_step.1 = (bf16[16,1024]{1,0:T(8,128)(2,1)S(1)}, bf16[16,288]{1,0:T(8,128)(2,1)S(1)}) custom-call(bf16[16,1024]{1,0:T(8,128)(2,1)} %refs_0_.1, bf16[16,1024,256]{2,1,0:T(8,128)(2,1)} %refs_1_.1, bf16[16,32,1024]{2,1,0:T(8,128)(2,1)} %bitcast.8, s32[4,16]{1,0:T(4,128)} %bitcast.12, f32[4,16]{1,0:T(4,128)} %bitcast.13, f32[1,1024]{1,0:T(1,128)} %bitcast.10, ...), custom_call_target="tpu_custom_call" | custom-call | tf_op jit(solution)/shard_map/decode_step/pallas_call | solution.py:513
  19.6 0.6 %store_step.1 = (bf16[16,1024]{1,0:T(8,128)(2,1)}, bf16[16,288]{1,0:T(8,128)(2,1)}) custom-call(bf16[16,1024]{1,0:T(8,128)(2,1)S(1)} %get-tuple-element.4.mixed_ref, bf16[16,288]{1,0:T(8,128)(2,1)S(1)} %get-tuple-element.5.entry_ref), custom_call_target="tpu_custom_call" | custom-call | tf_op jit(solution)/shard_map/store_step/pallas_call | solution.py:546

commit v4 on v3

--- a/solution.py
+++ b/solution.py
@@ -13,7 +13,6 @@
 ROPE = 32
 VDIM = 64
 CAP = 4
-GROUP = 4
 
 norm_eps = 1e-06
 masked_score = -1e30
@@ -45,6 +44,10 @@
 
 def onehot(cond):
     return jnp.where(cond, 1.0, 0.0).astype(BF16)
+
+
+def group_sizes(rows):
+    return [rows // 4, 3 * rows // 8, rows - rows // 4 - 3 * rows // 8]
 
 
 def step_kernel(ep_size, tp_size, names, *refs):
@@ -157,7 +160,7 @@
         landed(total, load_sem.at[batches.index(batch)])
 
     def cache_copies(g):
-        part = pl.ds(g * GROUP, GROUP)
+        part = pl.ds(members[g][0], len(members[g]))
         return (
             pltpu.make_async_copy(
                 hbm["latent_cache"].at[part], vmem["latent_cache"].at[part], cache_sem.at[g]
@@ -168,11 +171,14 @@
         )
 
     def cache_wait(g):
-        part = pl.ds(0, GROUP)
+        part = pl.ds(0, len(members[g]))
         total = size_of(hbm["latent_cache"].at[part]) + size_of(hbm["rope_cache"].at[part])
         landed(total, cache_sem.at[g])
 
-    groups = rows // GROUP
+    sizes = group_sizes(rows)
+    groups = len(sizes)
+    members = [range(sum(sizes[:g]), sum(sizes[: g + 1])) for g in range(groups)]
+
     def begin(g):
         if g < groups:
             for copy in cache_copies(g):
@@ -224,8 +230,8 @@
     tokens = vmem["tokens"][...].astype(F32)
     normed = rms(tokens, vmem["g_attn"][...]).astype(BF16)
     query_low = rms(nn(normed, vmem["w_query_down"][...]), vmem["g_query"][...]).astype(BF16)
+    finish(second)
     begin(2)
-    finish(second)
     query = nn(query_low, vmem["w_query"][...])
     turn = nn(query_low, vmem["w_query_rope"][...])
     rope_width = turn.shape[1]
@@ -257,16 +263,12 @@
     quad = span // NOPE
     quad_lane = iota((rows, span), 1) // NOPE
     w_key_up = vmem["w_key_up"]
-    for g in range(3, groups):
-        begin(g)
-    cache_wait(0)
+
+    cut = 3 * length // 4
 
     def turn_keys(s):
-        turned_ref[s % (2 * GROUP)] = vmem["latent_cache"][s].T
-
-    load(third)
-    for s in range(GROUP):
-        turn_keys(s)
+        turned_ref[s] = vmem["latent_cache"][s, 0:cut, :].T
+
     for n in range(HEADS // quad):
         piece = query[:, n * span : (n + 1) * span]
         spread_query = jnp.concatenate(
@@ -302,7 +304,10 @@
     def score(s):
         query_latent = get_wide(ql_ref, head_rows(s)).astype(BF16)
         query_rope = qr_ref[head_rows(s), :][:, 0:ROPE].astype(BF16)
-        found = nn(query_latent, turned_ref[s % (2 * GROUP)])
+        found = nn(query_latent, turned_ref[s])
+        if cut < length:
+            rest = nt(query_latent, vmem["latent_cache"][s, cut:length, :])
+            found = jnp.concatenate([found, rest], axis=1)
         return found + nn(query_rope, vmem["rope_cache"][s])
 
     def soften(s, scores):
@@ -316,30 +321,26 @@
         mixed = nn(weights, vmem["latent_cache"][s])
         put_wide(mix_ref, head_rows(s), mixed / total)
 
-    members = [range(g * GROUP, (g + 1) * GROUP) for g in range(groups)]
-    scored = []
-    for g in range(groups + 1):
-        if g + 1 < groups:
-            cache_wait(g + 1)
+    for g in range(groups):
+        cache_wait(g)
         if g == 0:
+            for later in range(3, groups):
+                begin(later)
+        if g == 0:
+            load(third)
+        if g == groups - 1:
             load(fourth)
             load(expert_names)
-        if g == max(groups - 2, 0):
-            pl.semaphore_wait(barrier, devices - 1)
-            for copy in swaps:
-                copy.start()
-        if g == max(groups - 1, 0):
-            finish(third)
-        soft = []
-        if g > 0:
-            soft = [soften(s, scores) for s, scores in zip(members[g - 1], scored)]
-        if g < groups:
-            scored = [score(s) for s in members[g]]
-        if g + 1 < groups:
-            for s in members[g + 1]:
-                turn_keys(s)
-        for s, (weights, total) in zip(members[g - 1], soft):
+        for s in members[g]:
+            turn_keys(s)
+        scored = [score(s) for s in members[g]]
+        soft = [soften(s, scores) for s, scores in zip(members[g], scored)]
+        for s, (weights, total) in zip(members[g], soft):
             mix(s, weights, total)
+    finish(third)
+    pl.semaphore_wait(barrier, devices - 1)
+    for copy in swaps:
+        copy.start()
     value_pieces = []
     for n in range(HEADS // quad):
         part = get_wide(mix_ref, pl.ds(n * quad * rows, quad * rows)).astype(BF16)
@@ -423,8 +424,8 @@
         copy.wait()
     gates, ups, downs = (vmem[name] for name in expert_names)
 
-    def serve(p):
-        steps = range(p * crew, (p + 1) * crew)
+    def serve(low, high):
+        steps = range(low * crew, high * crew)
         for e in range(own_experts):
             x = jnp.concatenate(
                 [inbox[s, e * CAP : (e + 1) * CAP, :] for s in steps], axis=0
@@ -434,7 +435,7 @@
             for i, s in enumerate(steps):
                 ret_out[s, e * CAP : (e + 1) * CAP, :] = total[i * CAP : (i + 1) * CAP, :]
 
-    for p in range(planes):
+    def collect(p):
         if crew > 1:
             gate = out_recv.at[2 * p + 1]
             bulk(inbox, p * crew + 1, crew - 1, send_sem.at[0], gate).wait_recv()
@@ -442,12 +443,21 @@
         @pl.when(plane != p)
         def _():
             bulk(inbox, p * crew, 1, send_sem.at[0], out_recv.at[2 * p]).wait_recv()
-        serve(p)
-        each(1, crew, lambda i: back(p, i).start())
-
+
+    def give(p):
         @pl.when(plane != p)
         def _():
             back(p, 0).start()
+
+        each(1, crew, lambda i: back(p, i).start())
+
+    chunks = ((0, 1), (1, 2), (2, 3), (3, 4))
+    for low, high in chunks if planes == 4 else [(0, planes)]:
+        for p in range(low, high):
+            collect(p)
+        serve(low, high)
+        for p in range(low, high):
+            give(p)
 
     ret_in[plane * crew] = ret_out[plane * crew]
     remote = devices - 1
@@ -523,7 +533,7 @@
             pltpu.VMEM((kvl // 128, pairs, 128), F32),
             pltpu.VMEM((pairs, 128), F32),
             pltpu.VMEM((kvl // 128, pairs, 128), F32),
-            pltpu.VMEM((2 * GROUP, kvl, length), BF16),
+            pltpu.VMEM((rows, kvl, 3 * length // 4), BF16),
             pltpu.VMEM((slots, rows), BF16),
             box,
             box,
@@ -531,7 +541,7 @@
             box,
             dma((7,)),
             dma((5,)),
-            dma((rows // GROUP,)),
+            dma((len(group_sizes(rows)),)),
             dma((3, max(tp_size - 1, 1))),
             dma((3, max(tp_size - 1, 1))),
             dma((2,)),

time: 20.3 us -> 19.7 us (0.970)
  Pallas kernels: 19.5 us -> 18.9 us
    pallas_call x1, Pallas kernels: 18.9 us -> 18.3 us  [local(): pl.pallas_call(functools.partial(step_kernel, ep_size, tp_size, NAMES), o...]
where the time goes in v4:
time: 19.7 us; the launch traced here: 19.6 us
  Pallas kernels  18.9 us (96%)
  between operations  0.65 us (3%)
    pallas_call x1, Pallas kernels, local(): pl.pallas_call(functools.partial(step_kernel, ep_size, tp_size, NAMES), o...  18.3 us
    pallas_call x1, Pallas kernels, local(): pl.pallas_call(store_kernel, out_shape=(jax.ShapeDtypeStruct(mixed.shape,...  0.64 us

profile of v4, /device:TPU:0, one launch (start us, length us, event | category | flops | bytes accessed | tf_op | source)
XLA Modules:
  0.0 19.6 jit_solution(2785763058816328451)
XLA Ops:
  0.6 18.3 %decode_step.1 = (bf16[16,1024]{1,0:T(8,128)(2,1)S(1)}, bf16[16,288]{1,0:T(8,128)(2,1)S(1)}) custom-call(bf16[16,1024]{1,0:T(8,128)(2,1)} %refs_0_.1, bf16[16,1024,256]{2,1,0:T(8,128)(2,1)} %refs_1_.1, bf16[16,32,1024]{2,1,0:T(8,128)(2,1)} %bitcast.8, s32[4,16]{1,0:T(4,128)} %bitcast.12, f32[4,16]{1,0:T(4,128)} %bitcast.13, f32[1,1024]{1,0:T(1,128)} %bitcast.10, ...), custom_call_target="tpu_custom_call" | custom-call | tf_op jit(solution)/shard_map/decode_step/pallas_call | solution.py:523
  19.0 0.6 %store_step.1 = (bf16[16,1024]{1,0:T(8,128)(2,1)}, bf16[16,288]{1,0:T(8,128)(2,1)}) custom-call(bf16[16,1024]{1,0:T(8,128)(2,1)S(1)} %get-tuple-element.4.mixed_ref, bf16[16,288]{1,0:T(8,128)(2,1)S(1)} %get-tuple-element.5.entry_ref), custom_call_target="tpu_custom_call" | custom-call | tf_op jit(solution)/shard_map/store_step/pallas_call | solution.py:556

commit v5 on v4

--- a/solution.py
+++ b/solution.py
@@ -116,7 +116,7 @@
         return vmem[name].at[:, :, part]
 
     small = (
-        "lengths", "expert_ids", "route_weights", "g_attn", "g_query", "g_latent", "g_ffn",
+        "g_attn", "g_query", "lengths", "expert_ids", "route_weights", "g_latent", "g_ffn",
     )
     first = ("tokens", "w_query_down")
     second = ("w_query", "w_query_rope", "w_key_up")
@@ -197,10 +197,18 @@
 
     load(second)
     begin(0)
-    for name in small:
-        load(name).wait()
+    load("g_attn").wait()
+    load("g_query").wait()
     finish(first)
     begin(1)
+    tokens = vmem["tokens"][...].astype(F32)
+    normed = rms(tokens, vmem["g_attn"][...]).astype(BF16)
+    query_low = rms(nn(normed, vmem["w_query_down"][...]), vmem["g_query"][...]).astype(BF16)
+    finish(second)
+    begin(2)
+    for name in small:
+        if name not in ("g_attn", "g_query"):
+            load(name).wait()
     lens = vmem["lengths"]
     ids = vmem["expert_ids"][...]
     slot = iota((slots, rows), 0)
@@ -227,11 +235,6 @@
     sine = jnp.sin(angle)
     sine = jnp.where((lane & (ROPE - 1)) < half, -sine, sine)
 
-    tokens = vmem["tokens"][...].astype(F32)
-    normed = rms(tokens, vmem["g_attn"][...]).astype(BF16)
-    query_low = rms(nn(normed, vmem["w_query_down"][...]), vmem["g_query"][...]).astype(BF16)
-    finish(second)
-    begin(2)
     query = nn(query_low, vmem["w_query"][...])
     turn = nn(query_low, vmem["w_query_rope"][...])
     rope_width = turn.shape[1]
@@ -264,10 +267,15 @@
     quad_lane = iota((rows, span), 1) // NOPE
     w_key_up = vmem["w_key_up"]
 
-    cut = 3 * length // 4
+    quarters = (0, 2, 4, 4, 3, 3)
+    cuts = {}
+    for group in members:
+        for i, s in enumerate(group):
+            cuts[s] = quarters[min(i, len(quarters) - 1)] * length // 4
 
     def turn_keys(s):
-        turned_ref[s] = vmem["latent_cache"][s, 0:cut, :].T
+        if cuts[s]:
+            turned_ref[s, :, 0 : cuts[s]] = vmem["latent_cache"][s, 0 : cuts[s], :].T
 
     for n in range(HEADS // quad):
         piece = query[:, n * span : (n + 1) * span]
@@ -304,17 +312,20 @@
     def score(s):
         query_latent = get_wide(ql_ref, head_rows(s)).astype(BF16)
         query_rope = qr_ref[head_rows(s), :][:, 0:ROPE].astype(BF16)
-        found = nn(query_latent, turned_ref[s])
+        cut = cuts[s]
+        pieces = []
+        if cut > 0:
+            pieces.append(nn(query_latent, turned_ref[s, :, 0:cut]))
         if cut < length:
-            rest = nt(query_latent, vmem["latent_cache"][s, cut:length, :])
-            found = jnp.concatenate([found, rest], axis=1)
+            pieces.append(nt(query_latent, vmem["latent_cache"][s, cut:length, :]))
+        found = pieces[0] if len(pieces) == 1 else jnp.concatenate(pieces, axis=1)
         return found + nn(query_rope, vmem["rope_cache"][s])
 
     def soften(s, scores):
         live = time_lane < lens[s]
         scores = jnp.where(live, scores * scale, masked_score)
         top = jnp.max(scores, axis=1, keepdims=True)
-        weights = jnp.where(live, jnp.exp(scores - top), 0.0)
+        weights = jnp.exp(scores - top)
         return weights.astype(BF16), jnp.sum(weights, axis=1, keepdims=True)
 
     def mix(s, weights, total):
@@ -533,7 +544,7 @@
             pltpu.VMEM((kvl // 128, pairs, 128), F32),
             pltpu.VMEM((pairs, 128), F32),
             pltpu.VMEM((kvl // 128, pairs, 128), F32),
-            pltpu.VMEM((rows, kvl, 3 * length // 4), BF16),
+            pltpu.VMEM((rows, kvl, length), BF16),
             pltpu.VMEM((slots, rows), BF16),
             box,
             box,

time: 19.7 us -> 19.6 us (level)
  no operation moved by 1% of the time
where the time goes in v5:
time: 19.6 us; the launch traced here: 19.4 us
  Pallas kernels  18.8 us (96%)
  between operations  0.65 us (3%)
    pallas_call x1, Pallas kernels, local(): pl.pallas_call(functools.partial(step_kernel, ep_size, tp_size, NAMES), o...  18.1 us
    pallas_call x1, Pallas kernels, local(): pl.pallas_call(store_kernel, out_shape=(jax.ShapeDtypeStruct(mixed.shape,...  0.64 us

profile of v5, /device:TPU:0, one launch (start us, length us, event | category | flops | bytes accessed | tf_op | source)
XLA Modules:
  0.0 19.4 jit_solution(5812686508317751273)
XLA Ops:
  0.6 18.1 %decode_step.1 = (bf16[16,1024]{1,0:T(8,128)(2,1)S(1)}, bf16[16,288]{1,0:T(8,128)(2,1)S(1)}) custom-call(bf16[16,1024]{1,0:T(8,128)(2,1)} %refs_0_.1, bf16[16,1024,256]{2,1,0:T(8,128)(2,1)} %refs_1_.1, bf16[16,32,1024]{2,1,0:T(8,128)(2,1)} %bitcast.8, s32[4,16]{1,0:T(4,128)} %bitcast.12, f32[4,16]{1,0:T(4,128)} %bitcast.13, f32[1,1024]{1,0:T(1,128)} %bitcast.10, ...), custom_call_target="tpu_custom_call" | custom-call | tf_op jit(solution)/shard_map/decode_step/pallas_call | solution.py:534
  18.8 0.6 %store_step.1 = (bf16[16,1024]{1,0:T(8,128)(2,1)}, bf16[16,288]{1,0:T(8,128)(2,1)}) custom-call(bf16[16,1024]{1,0:T(8,128)(2,1)S(1)} %get-tuple-element.4.mixed_ref, bf16[16,288]{1,0:T(8,128)(2,1)S(1)} %get-tuple-element.5.entry_ref), custom_call_target="tpu_custom_call" | custom-call | tf_op jit(solution)/shard_map/store_step/pallas_call | solution.py:567
